TPU v7x, 32 devices: a whole 2x2x4 slice. The times are simulated.
32 devices in a mesh: kv: 8 (over z, y), tp: 4 (over x, core).
Axes of the slice: x: 2, y: 2, z: 4, core: 2. Of those that a mesh axis runs over, the one named last changes fastest.
Arguments:
- tokens: bfloat16 [6144, 2048], P('kv'), may hold values from -6 to 6
- w_query: bfloat16 [2048, 4096], P(None, 'tp'), may hold values from -3.1819805 to 3.1819805
- w_latent: bfloat16 [2048, 256], replicated, may hold values from -0.13258252 to 0.13258252
- latent_gain: float32 [256], replicated, may hold values from 0.1 to 1.9
- w_output: bfloat16 [4096, 2048], P('tp'), may hold values from -2 to 2
- chosen: int32 [96, 32], P('kv'), may hold values from -1 to 95, as said below
Outputs:
- attended: bfloat16 [6144, 2048], P(('kv', 'tp'))
- log_total: float32 [6144, 16], P('kv', 'tp')
Inputs may be any that keep to these rules, and one draw needn't show every extreme that they name: `chosen`: row g names blocks at or before block g, no block twice; entry 0 is g itself; entries -1 name nothing and stand after the others. The 12 rows of one device together name exactly 2 distinct blocks of every earlier device's positions and none of a later device's.
All inputs are finite; a program needn't handle non-finite values.
Results may differ from a plain program's by a relative error of at most 0.01.
Values may be sent and summed in bfloat16 or wider, within the bound.
A program may use at most 192 MiB of HBM per device.

v0:
```python
import math

import jax
import jax.numpy as jnp
from jax import lax
from jax.sharding import PartitionSpec as P

CAP = 2


epsilon = 1e-06


def latents_of(tokens, w_latent, latent_gain):
    projected = jnp.dot(tokens, w_latent, preferred_element_type=jnp.float32)
    inv_rms = lax.rsqrt(jnp.mean(projected * projected, axis=-1, keepdims=True) + epsilon)
    return (projected * inv_rms * latent_gain).astype(jnp.bfloat16)


def attend(query_part, key_rows, picked, query_blocks, blk_len, score_scale):
    group_size, picks_each = picked.shape
    offsets = jnp.arange(blk_len, dtype=jnp.int32)
    key_pos = (picked[:, :, None] * blk_len + offsets[None, None, :]).reshape(
        group_size, picks_each * blk_len
    )
    usable = jnp.repeat(picked >= 0, blk_len, axis=1)
    query_pos = query_blocks[:, None] * blk_len + offsets[None, :]
    allowed = usable[:, None, :] & (key_pos[:, None, :] <= query_pos[:, :, None])
    scores = (
        jnp.einsum("gqhr,gkr->ghqk", query_part, key_rows, preferred_element_type=jnp.float32)
        * score_scale
    )
    scores = jnp.where(allowed[:, None, :, :], scores, -jnp.inf)
    peak_score = jnp.max(scores, axis=3, keepdims=True)
    raised = jnp.exp(scores - peak_score)
    total_mass = jnp.sum(raised, axis=3)
    weights = raised.astype(jnp.bfloat16)
    summed = jnp.einsum("ghqk,gkr->gqhr", weights, key_rows, preferred_element_type=jnp.float32)
    mass_t = jnp.transpose(total_mass, (0, 2, 1))
    heads_out = (summed / mass_t[..., None]).astype(jnp.bfloat16)
    log_part = jnp.transpose(peak_score[..., 0], (0, 2, 1)) + jnp.log(mass_t)
    return (heads_out, log_part)


def slot_table(hit_mask):
    counted = jnp.cumsum(hit_mask.astype(jnp.int32), axis=1) - 1
    slot_ids = jnp.arange(CAP, dtype=jnp.int32)
    match_mask = hit_mask[:, None, :] & (counted[:, None, :] == slot_ids[None, :, None])
    places = jnp.arange(hit_mask.shape[1], dtype=jnp.int32)
    found = jnp.sum(jnp.where(match_mask, places[None, None, :], 0), axis=2)
    slot_list = jnp.where(jnp.any(match_mask, axis=2), found, -1)
    return (counted, slot_list)


def local(tokens, w_query, w_latent, latent_gain, w_output, chosen):
    tok_rows = tokens.shape[0]
    lat_rank = w_latent.shape[1]
    head_count = w_query.shape[1] // lat_rank
    per_device, picks_each = chosen.shape
    blk_len = tok_rows // per_device
    devices = lax.axis_size("kv")
    my_index = lax.axis_index("kv")
    latent = latents_of(tokens, w_latent, latent_gain)
    safe_ids = jnp.maximum(chosen, 0)
    own_blocks = latent.reshape(per_device, blk_len, lat_rank)
    flat_ids = chosen.reshape(per_device * picks_each)
    every_block = jnp.arange(devices * per_device, dtype=jnp.int32)
    owners = jnp.arange(devices, dtype=jnp.int32)
    others = (owners != my_index)[:, None]
    wanted = (
        jnp.any(flat_ids[:, None] == every_block[None, :], axis=0).reshape(devices, per_device)
        & others
    )
    counted, request = slot_table(wanted)
    reply_blocks = jnp.take(
        own_blocks,
        jnp.maximum(lax.all_to_all(request, "kv", split_axis=0, concat_axis=0, tiled=True), 0),
        axis=0,
    )
    fetched = lax.all_to_all(reply_blocks, "kv", split_axis=0, concat_axis=0, tiled=True)
    key_table = jnp.concatenate(
        [own_blocks, fetched.reshape(devices * CAP, blk_len, lat_rank)], axis=0
    )
    owner_of = safe_ids // per_device
    rank_of = jnp.take(counted.reshape(devices * per_device), safe_ids)
    lookup = jnp.where(
        owner_of == my_index,
        safe_ids - my_index * per_device,
        per_device + owner_of * CAP + rank_of,
    )
    queries = jnp.dot(tokens, w_query, preferred_element_type=jnp.float32).astype(jnp.bfloat16)
    queries = queries.reshape(per_device, blk_len, head_count, lat_rank)
    group_size = math.gcd(per_device, max(1, 512 // (blk_len * head_count)))
    first_block = my_index * per_device
    score_scale = lat_rank ** (-0.5)

    def one_group(offset):
        picked = lax.dynamic_slice_in_dim(chosen, offset, group_size, 0)
        located = lax.dynamic_slice_in_dim(lookup, offset, group_size, 0)
        query_part = lax.dynamic_slice_in_dim(queries, offset, group_size, 0)
        key_rows = jnp.take(key_table, located, axis=0).reshape(
            group_size, picks_each * blk_len, lat_rank
        )
        query_blocks = first_block + offset + jnp.arange(group_size, dtype=jnp.int32)
        return attend(query_part, key_rows, picked, query_blocks, blk_len, score_scale)

    group_starts = jnp.arange(0, per_device, group_size, dtype=jnp.int32)
    heads_out, log_total = lax.map(one_group, group_starts)
    heads_flat = heads_out.reshape(tok_rows, head_count * lat_rank)
    log_total = log_total.reshape(tok_rows, head_count)
    attended = lax.psum_scatter(
        jnp.dot(heads_flat, w_output, preferred_element_type=jnp.float32).astype(jnp.bfloat16),
        "tp",
        scatter_dimension=0,
        tiled=True,
    )
    return (attended, log_total)


def solution(mesh):
    placed = (P("kv", None), P(None, "tp"), P(), P(), P("tp", None), P("kv", None))
    return jax.shard_map(
        local,
        mesh=mesh,
        in_specs=placed,
        out_specs=(P(("kv", "tp"), None), P("kv", "tp")),
        check_vma=False,
    )
```

profile of v0, /device:TPU:0, one launch (start us, length us, event | category | flops | bytes accessed | tf_op | source)
XLA Modules:
  0.0 218.4 jit_solution(2294472344887354751)
XLA Ops:
  9.6 7.3 %all-to-all-start = ((s32[8,1,2]{2,1,0:T(1,128)}), s32[8,1,2]{2,1,0:T(1,128)S(1)}, u32[]{:S(2)}, u32[]{:S(2)}) async-start(s32[8,1,2]{2,1,0:T(1,128)} %copy.23), calls=%async_computation | async-start | bytes 8192 | tf_op jit(solution)/shard_map/all_to_all | solution.py:77
  17.7 3.1 %multiply_reduce_fusion = (f32[768]{0:T(1024)S(1)}, f32[768,256]{1,0:T(8,128)}) fusion(bf16[768,2048]{1,0:T(8,128)(2,1)S(1)} %copy-done, bf16[2048,256]{1,0:T(8,128)(2,1)} %param.10), kind=kOutput, calls=%fused_computation.37 | convolution fusion | flops 805698816 | bytes 4983808 | tf_op jit(solution)/shard_map/dot_general | solution.py:15
  20.9 2.7 %gather_fusion.1 = s32[384]{0:T(512)S(1)} fusion(s32[96]{0:T(128)S(1)} %sub.30, s32[1024]{0:T(1024)S(1)} %pad_clamp_fusion.2), kind=kCustom, calls=%fused_computation.1 | custom fusion | bytes 4608 | tf_op jit(solution)/shard_map/jit(_take)/gather | solution.py:85
  32.2 6.0 %all-to-all-start.1 = ((bf16[8,2,64,256]{3,2,1,0:T(8,128)(2,1)}), bf16[8,2,64,256]{3,2,1,0:T(8,128)(2,1)}, u32[]{:S(2)}, u32[]{:S(2)}) async-start(bf16[8,2,64,256]{3,2,1,0:T(8,128)(2,1)} %broadcast_select_fusion), calls=%async_computation.1 | async-start | bytes 1048576 | tf_op jit(solution)/shard_map/all_to_all | solution.py:80
  38.2 6.7 %convolution_convert_fusion.1 = bf16[768,1024]{1,0:T(8,128)(2,1)} fusion(bf16[768,2048]{1,0:T(8,128)(2,1)S(1)} %copy-done, bf16[2048,1024]{1,0:T(8,128)(2,1)} %param.9), kind=kOutput, calls=%fused_computation.34 | convolution fusion | flops 3222011904 | bytes 8912896 | tf_op jit(solution)/shard_map/dot_general | solution.py:91
  44.9 3.9 %reshape.161 = bf16[12,64,4,256]{3,2,1,0:T(4,128)(2,1)} reshape(bf16[768,1024]{1,0:T(8,128)(2,1)} %convolution_convert_fusion.1) | data formatting | bytes 3145728 | tf_op jit(solution)/shard_map/reshape | solution.py:92
  54.3 111.4 %while.12 = (s32[]{:T(128)}, bf16[6,2,64,4,256]{4,3,2,1,0:T(4,128)(2,1)}, f32[6,2,64,4]{2,1,0,3:T(2,128)}, s32[6]{0:T(128)}, s32[12,32]{1,0:T(8,128)}, /*index=5...) while((s32[]{:T(128)}, ...), condition=%wide.region_8.9_spmd, body=%wide.region_5.8_spmd.sunk | while | flops 1082922112 | bytes 35847144 | solution.py:108
  58.3 3.2 %gather_fusion = bf16[64,64,256]{2,1,0:T(8,128)(2,1)} fusion(bf16[28,64,256]{2,1,0:T(8,128)(2,1)} %get-tuple-element.209, s32[1024]{0:T(1024)S(1)} %pad_clamp_fusion.4), kind=kCustom, calls=%fused_computation.clone.1 | custom fusion | bytes 4194560 | tf_op jit(solution)/shard_map/while/body/eval_jaxpr/jit(_take)/gather | solution.py:101
  61.6 2.9 %bitcast_select_fusion.3 = bf16[2,2048,256]{2,1,0:T(8,128)(2,1)} fusion(pred[2,2048]{1,0:T(4,128)(4,1)S(1)} %broadcast_in_dim.122, bf16[2,2048,256]{2,1,0:T(8,128)(2,1)} %bitcast.78), kind=kLoop, calls=%fused_computation.10.clone.1 | loop fusion | flops 1048576 | bytes 4198400 | tf_op jit(solution)/shard_map/while/body/eval_jaxpr/jit(_take)/select_n | solution.py:101
  67.0 2.6 %fusion.53 = (f32[2,4,64]{2,1,0:T(4,128)S(1)}, f32[2,4,64,2048]{3,2,1,0:T(8,128)S(1)}) fusion(bf16[2,64,4,256]{3,2,1,0:T(4,128)(2,1)S(1)} %constant_dynamic-slice_fusion.4, bf16[2,2048,256]{2,1,0:T(8,128)(2,1)} %bitcast_select_fusion.3, pred[2,64,2048]{2,1,0:T(8,128)(4,1)S(1)} %compare_and_fusion.5), kind=kOutput, calls=%fused_computation.62.clone.1 | convolution fusion | flops 540016128 | bytes 6817792 | tf_op jit(solution)/shard_map/while/body/eval_jaxpr/gqhr,gkr->ghqk/dot_general | solution.py:30
  76.8 3.2 %gather_fusion = bf16[64,64,256]{2,1,0:T(8,128)(2,1)} fusion(bf16[28,64,256]{2,1,0:T(8,128)(2,1)} %get-tuple-element.209, s32[1024]{0:T(1024)S(1)} %pad_clamp_fusion.4), kind=kCustom, calls=%fused_computation.clone.1 | custom fusion | bytes 4194560 | tf_op jit(solution)/shard_map/while/body/eval_jaxpr/jit(_take)/gather | solution.py:101
  80.2 2.9 %bitcast_select_fusion.3 = bf16[2,2048,256]{2,1,0:T(8,128)(2,1)} fusion(pred[2,2048]{1,0:T(4,128)(4,1)S(1)} %broadcast_in_dim.122, bf16[2,2048,256]{2,1,0:T(8,128)(2,1)} %bitcast.78), kind=kLoop, calls=%fused_computation.10.clone.1 | loop fusion | flops 1048576 | bytes 4198400 | tf_op jit(solution)/shard_map/while/body/eval_jaxpr/jit(_take)/select_n | solution.py:101
  95.4 3.2 %gather_fusion = bf16[64,64,256]{2,1,0:T(8,128)(2,1)} fusion(bf16[28,64,256]{2,1,0:T(8,128)(2,1)} %get-tuple-element.209, s32[1024]{0:T(1024)S(1)} %pad_clamp_fusion.4), kind=kCustom, calls=%fused_computation.clone.1 | custom fusion | bytes 4194560 | tf_op jit(solution)/shard_map/while/body/eval_jaxpr/jit(_take)/gather | solution.py:101
  98.7 2.9 %bitcast_select_fusion.3 = bf16[2,2048,256]{2,1,0:T(8,128)(2,1)} fusion(pred[2,2048]{1,0:T(4,128)(4,1)S(1)} %broadcast_in_dim.122, bf16[2,2048,256]{2,1,0:T(8,128)(2,1)} %bitcast.78), kind=kLoop, calls=%fused_computation.10.clone.1 | loop fusion | flops 1048576 | bytes 4198400 | tf_op jit(solution)/shard_map/while/body/eval_jaxpr/jit(_take)/select_n | solution.py:101
  114.0 3.2 %gather_fusion = bf16[64,64,256]{2,1,0:T(8,128)(2,1)} fusion(bf16[28,64,256]{2,1,0:T(8,128)(2,1)} %get-tuple-element.209, s32[1024]{0:T(1024)S(1)} %pad_clamp_fusion.4), kind=kCustom, calls=%fused_computation.clone.1 | custom fusion | bytes 4194560 | tf_op jit(solution)/shard_map/while/body/eval_jaxpr/jit(_take)/gather | solution.py:101
  117.3 2.9 %bitcast_select_fusion.3 = bf16[2,2048,256]{2,1,0:T(8,128)(2,1)} fusion(pred[2,2048]{1,0:T(4,128)(4,1)S(1)} %broadcast_in_dim.122, bf16[2,2048,256]{2,1,0:T(8,128)(2,1)} %bitcast.78), kind=kLoop, calls=%fused_computation.10.clone.1 | loop fusion | flops 1048576 | bytes 4198400 | tf_op jit(solution)/shard_map/while/body/eval_jaxpr/jit(_take)/select_n | solution.py:101
  122.7 2.6 %fusion.53 = (f32[2,4,64]{2,1,0:T(4,128)S(1)}, f32[2,4,64,2048]{3,2,1,0:T(8,128)S(1)}) fusion(bf16[2,64,4,256]{3,2,1,0:T(4,128)(2,1)S(1)} %constant_dynamic-slice_fusion.4, bf16[2,2048,256]{2,1,0:T(8,128)(2,1)} %bitcast_select_fusion.3, pred[2,64,2048]{2,1,0:T(8,128)(4,1)S(1)} %compare_and_fusion.5), kind=kOutput, calls=%fused_computation.62.clone.1 | convolution fusion | flops 540016128 | bytes 6817792 | tf_op jit(solution)/shard_map/while/body/eval_jaxpr/gqhr,gkr->ghqk/dot_general | solution.py:30
  132.5 3.2 %gather_fusion = bf16[64,64,256]{2,1,0:T(8,128)(2,1)} fusion(bf16[28,64,256]{2,1,0:T(8,128)(2,1)} %get-tuple-element.209, s32[1024]{0:T(1024)S(1)} %pad_clamp_fusion.4), kind=kCustom, calls=%fused_computation.clone.1 | custom fusion | bytes 4194560 | tf_op jit(solution)/shard_map/while/body/eval_jaxpr/jit(_take)/gather | solution.py:101
  135.8 2.9 %bitcast_select_fusion.3 = bf16[2,2048,256]{2,1,0:T(8,128)(2,1)} fusion(pred[2,2048]{1,0:T(4,128)(4,1)S(1)} %broadcast_in_dim.122, bf16[2,2048,256]{2,1,0:T(8,128)(2,1)} %bitcast.78), kind=kLoop, calls=%fused_computation.10.clone.1 | loop fusion | flops 1048576 | bytes 4198400 | tf_op jit(solution)/shard_map/while/body/eval_jaxpr/jit(_take)/select_n | solution.py:101
  141.3 2.6 %fusion.53 = (f32[2,4,64]{2,1,0:T(4,128)S(1)}, f32[2,4,64,2048]{3,2,1,0:T(8,128)S(1)}) fusion(bf16[2,64,4,256]{3,2,1,0:T(4,128)(2,1)S(1)} %constant_dynamic-slice_fusion.4, bf16[2,2048,256]{2,1,0:T(8,128)(2,1)} %bitcast_select_fusion.3, pred[2,64,2048]{2,1,0:T(8,128)(4,1)S(1)} %compare_and_fusion.5), kind=kOutput, calls=%fused_computation.62.clone.1 | convolution fusion | flops 540016128 | bytes 6817792 | tf_op jit(solution)/shard_map/while/body/eval_jaxpr/gqhr,gkr->ghqk/dot_general | solution.py:30
  151.1 3.2 %gather_fusion = bf16[64,64,256]{2,1,0:T(8,128)(2,1)} fusion(bf16[28,64,256]{2,1,0:T(8,128)(2,1)} %get-tuple-element.209, s32[1024]{0:T(1024)S(1)} %pad_clamp_fusion.4), kind=kCustom, calls=%fused_computation.clone.1 | custom fusion | bytes 4194560 | tf_op jit(solution)/shard_map/while/body/eval_jaxpr/jit(_take)/gather | solution.py:101
  154.4 2.9 %bitcast_select_fusion.3 = bf16[2,2048,256]{2,1,0:T(8,128)(2,1)} fusion(pred[2,2048]{1,0:T(4,128)(4,1)S(1)} %broadcast_in_dim.122, bf16[2,2048,256]{2,1,0:T(8,128)(2,1)} %bitcast.78), kind=kLoop, calls=%fused_computation.10.clone.1 | loop fusion | flops 1048576 | bytes 4198400 | tf_op jit(solution)/shard_map/while/body/eval_jaxpr/jit(_take)/select_n | solution.py:101
  167.5 7.0 %convolution_convert_fusion = bf16[768,2048]{1,0:T(8,128)(2,1)} fusion(bf16[768,1024]{1,0:T(8,128)(2,1)S(1)} %bitcast.82, bf16[1024,2048]{1,0:T(8,128)(2,1)} %param.12), kind=kOutput, calls=%fused_computation.33 | convolution fusion | flops 3222798336 | bytes 8912896 | tf_op jit(solution)/shard_map/dot_general | solution.py:112
  175.8 35.7 %reduce-scatter.2.cloned.1.call-done = bf16[192,2048]{1,0:T(8,128)(2,1)} async-done(((bf16[768,2048]{1,0:T(8,128)(2,1)}), bf16[192,2048]{1,0:T(8,128)(2,1)}) %reduce-scatter.2.cloned.1.call-update) | async-done | bytes 786448 | tf_op jit(solution)/shard_map/reduce_scatter | solution.py:111
  (196 shorter events, 71.7 us)
Async XLA Ops:
  7.2 10.5 %copy-start = (bf16[768,2048]{1,0:T(8,128)(2,1)S(1)}, bf16[768,2048]{1,0:T(8,128)(2,1)}, u32[]{:S(2)}) copy-start(bf16[768,2048]{1,0:T(8,128)(2,1)} %param.8) | copy-start | bytes 9437188
  9.6 15.4 %all-to-all-start = ((s32[8,1,2]{2,1,0:T(1,128)}), s32[8,1,2]{2,1,0:T(1,128)S(1)}, u32[]{:S(2)}, u32[]{:S(2)}) async-start(s32[8,1,2]{2,1,0:T(1,128)} %copy.23), calls=%async_computation | async-start | bytes 8192 | tf_op jit(solution)/shard_map/all_to_all | solution.py:77
  32.2 20.1 %all-to-all-start.1 = ((bf16[8,2,64,256]{3,2,1,0:T(8,128)(2,1)}), bf16[8,2,64,256]{3,2,1,0:T(8,128)(2,1)}, u32[]{:S(2)}, u32[]{:S(2)}) async-start(bf16[8,2,64,256]{3,2,1,0:T(8,128)(2,1)} %broadcast_select_fusion), calls=%async_computation.1 | async-start | bytes 1048576 | tf_op jit(solution)/shard_map/all_to_all | solution.py:80
  38.2 173.3 %reduce-scatter.2.cloned.1.call-start = ((), (), s32[]{:S(2)}) async-start(), calls=%async_computation.3 | async-start | bytes 3932160 | tf_op jit(solution)/shard_map/reduce_scatter | solution.py:111
  44.9 4.4 %copy-start.2 = (s32[12,32]{1,0:T(8,128)S(1)}, s32[12,32]{1,0:T(8,128)}, u32[]{:S(2)}) copy-start(s32[12,32]{1,0:T(8,128)} %param.13) | copy-start | bytes 4612
  69.6 1.6 copy-start.1
  88.1 1.6 copy-start.1
  106.7 1.6 copy-start.1
  125.3 1.6 copy-start.1
  143.8 1.6 copy-start.1
  162.4 1.6 copy-start.1
  174.4 0.7 copy-start.3
Sparse Core Ops, SparseCore 0:
  174.6 36.9 reduce-scatter.1
where the time goes:
time: 221 us; the launch traced here: 218 us
  local copies, waits for them, and re-layouts  62.8 us (28%)
  waiting for transfers between devices  38 us (17%)
  other arithmetic  37.4 us (17%)
  matrix products  36.7 us (17%)
  loops' own time  16 us (7%)
  between operations  14.1 us (6%)
  starting transfers between devices  13.3 us (6%)
    reduce_scatter x1, waiting for transfers between devices, local(): lax.psum_scatter(jnp.dot(heads_flat, w_output, preferred_element_type=jnp...  35.7 us
    gather x6, local copies, waits for them, and re-layouts, one_group(): jnp.take(key_table, located, axis=0)  18.9 us
    select_n x6, other arithmetic, one_group(): jnp.take(key_table, located, axis=0)  17.6 us
    another operation x1, loops' own time, local(): heads_out, log_total = lax.map(one_group, group_starts)  16 us
    dot_general x6, matrix products, attend(): jnp.einsum('gqhr,gkr->ghqk', query_part, key_rows, preferred_element_type...  15.4 us
    dynamic_update_slice x12, local copies, waits for them, and re-layouts, local(): heads_out, log_total = lax.map(one_group, group_starts)  9.13 us
    all_to_all x1, starting transfers between devices, local(): lax.all_to_all(request, 'kv', split_axis=0, concat_axis=0, tiled=True)  7.31 us
    dynamic_slice x6, local copies, waits for them, and re-layouts, local(): heads_out, log_total = lax.map(one_group, group_starts)  7.2 us
  transfers between devices with their start and end apart: 3, of which 2 were waited for; matrix products, arithmetic and copies ran while one was open for 9% of the time, Pallas kernels for 0%

commit v1 on v0

v1 whole, which is shorter than its diff:
```python
import functools

import jax
import jax.numpy as jnp
from jax import lax
from jax.experimental import pallas as pl
from jax.experimental.pallas import tpu as pltpu
from jax.sharding import PartitionSpec as P

CAP = 2
PAIR = 2
FAR = 1 << 30
LOG2E = 1.4426950408889634

epsilon = 1e-06


def latents_of(tokens, w_latent, latent_gain):
    projected = jnp.dot(tokens, w_latent, preferred_element_type=jnp.float32)
    inv_rms = lax.rsqrt(jnp.mean(projected * projected, axis=-1, keepdims=True) + epsilon)
    return (projected * inv_rms * latent_gain).astype(jnp.bfloat16)


def slot_table(hit_mask):
    counted = jnp.cumsum(hit_mask.astype(jnp.int32), axis=1) - 1
    slot_ids = jnp.arange(CAP, dtype=jnp.int32)
    match_mask = hit_mask[:, None, :] & (counted[:, None, :] == slot_ids[None, :, None])
    places = jnp.arange(hit_mask.shape[1], dtype=jnp.int32)
    found = jnp.sum(jnp.where(match_mask, places[None, None, :], 0), axis=2)
    return jnp.where(jnp.any(match_mask, axis=2), found, -1)


def attend_kernel(
    n_tp, blk, heads, rank, per_shard,
    q_ref, key_ref, pos_ref, w_ref, out_ref, log_ref,
    heads_buf, own, a_send, a_recv, x_send, x_recv, a_ss, a_rs, x_ss, x_rs,
):
    me = lax.axis_index("tp")
    pair, core = me // PAIR, me % PAIR
    groups = n_tp // PAIR
    partner = pair * PAIR + (PAIR - 1 - core)
    steps = groups * per_shard
    scale = rank ** (-0.5)
    factor = scale * LOG2E

    barrier = pltpu.get_barrier_semaphore()
    pl.semaphore_signal(barrier, inc=1, device_id={"tp": partner})
    for o in range(1, groups):
        pl.semaphore_signal(
            barrier, inc=1, device_id={"tp": lax.rem(pair + o, groups) * PAIR + core}
        )
    pl.semaphore_wait(barrier, groups)

    def near(s):
        return pltpu.make_async_remote_copy(
            src_ref=a_send.at[s], dst_ref=a_recv.at[s],
            send_sem=a_ss.at[s], recv_sem=a_rs.at[s], device_id={"tp": partner},
        )

    def cross(s):
        peer = lax.rem(pair + 1 + s // per_shard, groups) * PAIR + core
        return pltpu.make_async_remote_copy(
            src_ref=x_send.at[s], dst_ref=x_recv.at[s],
            send_sem=x_ss.at[s], recv_sem=x_rs.at[s], device_id={"tp": peer},
        )

    def attend(g, half):
        row0 = pl.multiple_of(g * blk, blk)
        q = jnp.concatenate(
            [q_ref[pl.ds(row0, blk), h * rank:(h + 1) * rank] for h in range(heads)], axis=0
        )
        keys = key_ref[...]
        s = lax.dot_general(q, keys, (((1,), (1,)), ((), ())), preferred_element_type=jnp.float32)
        pos = pos_ref[pl.ds(g, 1), :]
        query_pos = g * blk + lax.rem(
            lax.broadcasted_iota(jnp.int32, (heads * blk, 1), 0), jnp.int32(blk)
        )
        s = jnp.where(pos <= query_pos, s, -jnp.inf)
        peak = jnp.max(s, axis=1, keepdims=True)
        p = jnp.exp2((s - peak) * factor)
        mass = jnp.sum(p, axis=1, keepdims=True)
        summed = jnp.dot(p.astype(jnp.bfloat16), keys, preferred_element_type=jnp.float32)
        result = (summed / mass).astype(jnp.bfloat16)
        logs = peak * scale + jnp.log(mass)
        for h in range(heads):
            heads_buf[half * blk:(half + 1) * blk, h * rank:(h + 1) * rank] = (
                result[h * blk:(h + 1) * blk]
            )
        log_ref[pl.ds(row0, blk), :] = jnp.concatenate(
            [logs[h * blk:(h + 1) * blk] for h in range(heads)], axis=1
        )

    def finish(s):
        near(s).wait_recv()
        total = own[s] + a_recv[s].astype(jnp.float32)

        @pl.when(s < steps - per_shard)
        def _():
            x_send[s] = total.astype(jnp.bfloat16)
            cross(s).start()

        @pl.when(s >= steps - per_shard)
        def _():
            own[s] = total

    def step(s, carry):
        group = lax.rem(pair + 1 + s // per_shard, groups)
        inner = lax.rem(s, per_shard)
        attend((group * PAIR + (PAIR - 1 - core)) * per_shard + inner, 0)
        attend((group * PAIR + core) * per_shard + inner, 1)
        part = jnp.dot(heads_buf[...], w_ref[...], preferred_element_type=jnp.float32)
        a_send[s] = part[:blk].astype(jnp.bfloat16)
        own[s] = part[blk:]
        near(s).start()

        @pl.when(s >= 1)
        def _():
            finish(s - 1)

        return carry

    lax.fori_loop(0, steps, step, 0)
    finish(steps - 1)
    for i in range(per_shard):
        total = own[steps - per_shard + i]
        for o in range(groups - 1):
            slot = o * per_shard + i
            cross(slot).wait_recv()
            total = total + x_recv[slot].astype(jnp.float32)
        out_ref[i * blk:(i + 1) * blk, :] = total.astype(jnp.bfloat16)
    for s in range(steps):
        near(s).wait_send()
    for s in range(steps - per_shard):
        cross(s).wait_send()


def attend_and_reduce(queries, keys, positions, w_output, blk, rank):
    rows, width = queries.shape[0], w_output.shape[1]
    heads = queries.shape[1] // rank
    n_tp = lax.axis_size("tp")
    per_shard = rows // (n_tp * blk)
    steps = (n_tp // PAIR) * per_shard
    crossing = steps - per_shard
    return pl.pallas_call(
        functools.partial(attend_kernel, n_tp, blk, heads, rank, per_shard),
        out_shape=(
            jax.ShapeDtypeStruct((rows // n_tp, width), jnp.bfloat16),
            jax.ShapeDtypeStruct((rows, heads), jnp.float32),
        ),
        in_specs=[pl.BlockSpec(memory_space=pltpu.VMEM)] * 4,
        out_specs=[pl.BlockSpec(memory_space=pltpu.VMEM)] * 2,
        scratch_shapes=[
            pltpu.VMEM((PAIR * blk, heads * rank), jnp.bfloat16),
            pltpu.VMEM((steps, blk, width), jnp.float32),
            pltpu.VMEM((steps, blk, width), jnp.bfloat16),
            pltpu.VMEM((steps, blk, width), jnp.bfloat16),
            pltpu.VMEM((crossing, blk, width), jnp.bfloat16),
            pltpu.VMEM((crossing, blk, width), jnp.bfloat16),
            pltpu.SemaphoreType.DMA((steps,)),
            pltpu.SemaphoreType.DMA((steps,)),
            pltpu.SemaphoreType.DMA((crossing,)),
            pltpu.SemaphoreType.DMA((crossing,)),
        ],
        compiler_params=pltpu.CompilerParams(
            collective_id=0, has_side_effects=True, vmem_limit_bytes=56 * 1024 * 1024
        ),
    )(queries, keys, positions, w_output)


def local(tokens, w_query, w_latent, latent_gain, w_output, chosen):
    tok_rows = tokens.shape[0]
    lat_rank = w_latent.shape[1]
    per_device, picks_each = chosen.shape
    blk_len = tok_rows // per_device
    devices = lax.axis_size("kv")
    my_index = lax.axis_index("kv")
    every_block = jnp.arange(devices * per_device, dtype=jnp.int32)
    owners = jnp.arange(devices, dtype=jnp.int32)
    named = jnp.any(chosen[:, :, None] == every_block[None, None, :], axis=1)
    wanted = jnp.any(named, axis=0).reshape(devices, per_device)
    request = slot_table(wanted & (owners != my_index)[:, None])
    asked = lax.all_to_all(request, "kv", split_axis=0, concat_axis=0, tiled=True)
    latent = latents_of(tokens, w_latent, latent_gain)
    own_blocks = latent.reshape(per_device, blk_len, lat_rank)
    reply_blocks = jnp.take(own_blocks, jnp.maximum(asked, 0), axis=0)
    fetched = lax.all_to_all(reply_blocks, "kv", split_axis=0, concat_axis=0, tiled=True)
    keys = jnp.concatenate(
        [latent, fetched.reshape(devices * CAP * blk_len, lat_rank)], axis=0
    )
    queries = jnp.dot(tokens, w_query, preferred_element_type=jnp.float32).astype(jnp.bfloat16)

    own_ids = my_index * per_device + jnp.arange(per_device, dtype=jnp.int32)
    far_ids = jnp.where(request >= 0, owners[:, None] * per_device + request, -2).reshape(-1)
    slot_ids = jnp.concatenate([own_ids, far_ids])
    slot_named = jnp.any(chosen[:, :, None] == slot_ids[None, None, :], axis=1)
    key_named = jnp.repeat(slot_named, blk_len, axis=1)
    key_place = jnp.concatenate(
        [
            jnp.arange(tok_rows, dtype=jnp.int32),
            jnp.full((devices * CAP * blk_len,), -1, jnp.int32),
        ]
    )
    positions = jnp.where(key_named, key_place[None, :], FAR)
    return attend_and_reduce(queries, keys, positions, w_output, blk_len, lat_rank)


def solution(mesh):
    placed = (P("kv", None), P(None, "tp"), P(), P(), P("tp", None), P("kv", None))
    return jax.shard_map(
        local,
        mesh=mesh,
        in_specs=placed,
        out_specs=(P(("kv", "tp"), None), P("kv", "tp")),
        check_vma=False,
    )
```

time: 221 us -> 77.3 us (0.35)
  local copies, waits for them, and re-layouts: 62.8 us -> 9.22 us
  waiting for transfers between devices: 38 us -> 6.52 us
  Pallas kernels: 0 us -> 29.7 us
  other arithmetic: 37.4 us -> 8.7 us
  matrix products: 36.7 us -> 8.97 us
  loops' own time: 16 us -> 0 us
  between operations: 14.1 us -> 0.75 us
    reduce_scatter x1 -> x0, waiting for transfers between devices: 35.7 us -> none  [local(): lax.psum_scatter(jnp.dot(heads_flat, w_output, preferred_element_type=jnp...]
    pallas_call x0 -> x1, Pallas kernels: none -> 29.7 us  [attend_and_reduce(): pl.pallas_call(functools.partial(attend_kernel, n_tp, blk, heads, rank, p...]
    dot_general x13 -> x0, matrix products: 26.9 us -> none  [the longest x6 15.4 us: attend(): jnp.einsum('gqhr,gkr->ghqk', query_part, key_rows, preferred_element_type...]
    gather x9 -> x1, local copies, waits for them, and re-layouts: 23 us -> 1.37 us  [local(): reply_blocks = jnp.take(own_blocks, jnp.maximum(asked, 0), axis=0)]
    select_n x9 -> x3, other arithmetic: 20.2 us -> 3.35 us  [the longest x1 1.95 us: local(): reply_blocks = jnp.take(own_blocks, jnp.maximum(asked, 0), axis=0)]
    another operation x1 -> x0, loops' own time: 16 us -> none  [local(): heads_out, log_total = lax.map(one_group, group_starts)]
    dynamic_slice x12 -> x0, local copies, waits for them, and re-layouts: 13.5 us -> none  [the longest x6 7.2 us: local(): heads_out, log_total = lax.map(one_group, group_starts)]
    dynamic_update_slice x12 -> x0, local copies, waits for them, and re-layouts: 9.13 us -> none  [local(): heads_out, log_total = lax.map(one_group, group_starts)]
  transfers between devices with their start and end apart: 3 -> 2, of which waited for: 2 -> 2; matrix products, arithmetic and copies ran while one was open for 9% -> 18% of each run, Pallas kernels for 0% -> 0%
where the time goes in v1:
time: 77.3 us; the launch traced here: 76.6 us
  Pallas kernels  29.7 us (38%)
  starting transfers between devices  12.8 us (17%)
  local copies, waits for them, and re-layouts  9.22 us (12%)
  matrix products  8.97 us (12%)
  other arithmetic  8.7 us (11%)
  waiting for transfers between devices  6.52 us (8%)
    pallas_call x1, Pallas kernels, attend_and_reduce(): pl.pallas_call(functools.partial(attend_kernel, n_tp, blk, heads, rank, p...  29.7 us
    all_to_all x1, starting transfers between devices, local(): lax.all_to_all(request, 'kv', split_axis=0, concat_axis=0, tiled=True)  7.31 us
    dot_general x1, matrix products, local(): jnp.dot(tokens, w_query, preferred_element_type=jnp.float32)  6.68 us
    all_to_all x1, waiting for transfers between devices, local(): lax.all_to_all(reply_blocks, 'kv', split_axis=0, concat_axis=0, tiled=True)  5.99 us
    all_to_all x1, starting transfers between devices, local(): lax.all_to_all(reply_blocks, 'kv', split_axis=0, concat_axis=0, tiled=True)  5.46 us
    dot_general x1, matrix products, latents_of(): projected = jnp.dot(tokens, w_latent, preferred_element_type=jnp.float32)  2.29 us
    unnamed x7, local copies, waits for them, and re-layouts  2.11 us
    concatenate x1, other arithmetic, local(): jnp.concatenate([latent, fetched.reshape(devices * CAP * blk_len, lat_ran...  2.03 us
  transfers between devices with their start and end apart: 2, of which 2 were waited for; matrix products, arithmetic and copies ran while one was open for 18% of the time, Pallas kernels for 0%

profile of v1, /device:TPU:0, one launch (start us, length us, event | category | flops | bytes accessed | tf_op | source)
XLA Modules:
  0.0 76.6 jit_solution(370750413163799121)
XLA Ops:
  0.7 1.0 %fusion = pred[96]{0:T(512)(128)(4,1)S(1)} fusion(s32[12,32]{1,0:T(8,128)} %param.11), kind=kLoop, calls=%fused_computation.7 | loop fusion | flops 73632 | bytes 1632 | tf_op jit(solution)/shard_map/reduce_or | solution.py:180
  1.8 0.2 reduce_window_sum.11
  2.0 0.2 fusion.2
  2.1 0.2 select_reduce_fusion
  2.3 0.7 copy.21
  3.0 7.3 %all-to-all-start = ((s32[8,1,2]{2,1,0:T(1,128)}), s32[8,1,2]{2,1,0:T(1,128)S(1)}, u32[]{:S(2)}, u32[]{:S(2)}) async-start(s32[8,1,2]{2,1,0:T(1,128)} %copy.21), calls=%async_computation | async-start | bytes 8192 | tf_op jit(solution)/shard_map/all_to_all | solution.py:182
  10.6 0.8 %compare_reduce_fusion = pred[12,28]{1,0:T(8,128)(4,1)S(1)} fusion(s32[28]{0:T(128)S(1)} %pad_add_fusion, s32[12,32]{1,0:T(8,128)} %param.11), kind=kLoop, calls=%fused_computation.8 | loop fusion | flops 21168 | bytes 1984 | tf_op jit(solution)/shard_map/reduce_or | solution.py:195
  11.4 2.3 %multiply_reduce_fusion = (f32[768]{0:T(1024)S(1)}, f32[768,256]{1,0:T(8,128)S(1)}) fusion(bf16[768,2048]{1,0:T(8,128)(2,1)S(1)} %copy-done, bf16[2048,256]{1,0:T(8,128)(2,1)} %param.8), kind=kOutput, calls=%fused_computation.4 | convolution fusion | flops 805698816 | bytes 4983808 | tf_op jit(solution)/shard_map/dot_general | solution.py:19
  13.7 0.2 multiply_convert_fusion
  13.9 0.7 broadcast_in_dim.64
  14.7 1.5 %reshape.125 = pred[12,1792]{1,0:T(8,128)(4,1)} reshape(pred[12,28,64]{2,1,0:T(8,128)(4,1)} %broadcast_in_dim.64) | data formatting | bytes 43008 | tf_op jit(solution)/shard_map/reshape | solution.py:196
  16.2 0.5 all-to-all-done
  16.7 0.6 reshape.128
  17.6 0.7 pad_clamp_fusion
  18.2 1.4 %gather_fusion = bf16[16,64,256]{2,1,0:T(8,128)(2,1)} fusion(bf16[12,64,256]{2,1,0:T(8,128)(2,1)S(1)} %bitcast.10, s32[1024]{0:T(1024)S(1)} %pad_clamp_fusion), kind=kCustom, calls=%fused_computation | custom fusion | bytes 1048640 | tf_op jit(solution)/shard_map/jit(_take)/gather | solution.py:185
  19.6 1.9 %broadcast_select_fusion = bf16[8,2,64,256]{3,2,1,0:T(8,128)(2,1)} fusion(bf16[8,2,64,256]{3,2,1,0:T(8,128)(2,1)} %bitcast.11, pred[8,2]{1,0:T(8,128)(4,1)S(1)} %copy.23), kind=kLoop, calls=%fused_computation.5 | loop fusion | flops 262144 | bytes 1048592 | tf_op jit(solution)/shard_map/jit(_take)/select_n | solution.py:185
  21.5 5.5 %all-to-all-start.1 = ((bf16[8,2,64,256]{3,2,1,0:T(8,128)(2,1)}), bf16[8,2,64,256]{3,2,1,0:T(8,128)(2,1)}, u32[]{:S(2)}, u32[]{:S(2)}) async-start(bf16[8,2,64,256]{3,2,1,0:T(8,128)(2,1)} %broadcast_select_fusion), calls=%async_computation.1 | async-start | bytes 1048576 | tf_op jit(solution)/shard_map/all_to_all | solution.py:186
  27.0 1.4 %broadcast_select_fusion.1.pos_ref = s32[12,1792]{1,0:T(8,128)} fusion(pred[12,1792]{1,0:T(8,128)(4,1)} %reshape.125, s32[1792]{0:T(1024)S(1)} %copy-done.1), kind=kLoop, calls=%fused_computation.9 | loop fusion | flops 21504 | bytes 114688 | tf_op jit(solution)/shard_map/jit(_where)/select_n | solution.py:203
  28.4 6.7 %convolution_convert_fusion.q_ref = bf16[768,1024]{1,0:T(8,128)(2,1)} fusion(bf16[768,2048]{1,0:T(8,128)(2,1)S(1)} %copy-done, bf16[2048,1024]{1,0:T(8,128)(2,1)} %param.7), kind=kOutput, calls=%fused_computation.1 | convolution fusion | flops 3222011904 | bytes 8912896 | tf_op jit(solution)/shard_map/dot_general | solution.py:190
  35.1 6.0 %all-to-all-done.1 = bf16[8,2,64,256]{3,2,1,0:T(8,128)(2,1)} async-done(((bf16[8,2,64,256]{3,2,1,0:T(8,128)(2,1)}), bf16[8,2,64,256]{3,2,1,0:T(8,128)(2,1)}, u32[]{:S(2)}, u32[]{:S(2)}) %all-to-all-start.1) | async-done | bytes 524320 | tf_op jit(solution)/shard_map/all_to_all | solution.py:186
  41.1 2.0 %pad_maximum_fusion.key_ref = bf16[1792,256]{1,0:T(8,128)(2,1)} fusion(bf16[1024,256]{1,0:T(8,128)(2,1)} %bitcast.4, bf16[768,256]{1,0:T(8,128)(2,1)S(1)} %multiply_convert_fusion), kind=kLoop, calls=%fused_computation.2 | loop fusion | flops 1835008 | bytes 1835008 | tf_op jit(solution)/shard_map/concatenate | solution.py:187
  43.1 29.7 %shard_map.77 = (bf16[192,2048]{1,0:T(8,128)(2,1)}, f32[768,4]{1,0:T(8,128)}) custom-call(bf16[768,1024]{1,0:T(8,128)(2,1)} %convolution_convert_fusion.q_ref, bf16[1792,256]{1,0:T(8,128)(2,1)} %pad_maximum_fusion.key_ref, s32[12,1792]{1,0:T(8,128)} %broadcast_select_fusion.1.pos_ref, bf16[1024,2048]{1,0:T(8,128)(2,1)} %w_ref.1), custom_call_target="tpu_custom_call" | custom-call | tf_op jit(solution)/shard_map/pallas_call | solution.py:144
  72.8 1.7 %copy.25 = f32[768,4]{0,1:T(4,128)} copy(f32[768,4]{1,0:T(8,128)} %get-tuple-element.9) | data formatting | bytes 24576 | tf_op jit(solution)/shard_map/pallas_call | solution.py:144
  74.6 2.1 %copy.27 = bf16[192,2048]{1,0:T(8,128)(2,1)} copy(bf16[192,2048]{1,0:T(8,128)(2,1)} %get-tuple-element.18) | data formatting | bytes 1572864
  (21 shorter events, 0.7 us)
Async XLA Ops:
  0.6 10.8 %copy-start = (bf16[768,2048]{1,0:T(8,128)(2,1)S(1)}, bf16[768,2048]{1,0:T(8,128)(2,1)}, u32[]{:S(2)}) copy-start(bf16[768,2048]{1,0:T(8,128)(2,1)} %param.6) | copy-start | bytes 9437188
  3.0 13.7 %all-to-all-start = ((s32[8,1,2]{2,1,0:T(1,128)}), s32[8,1,2]{2,1,0:T(1,128)S(1)}, u32[]{:S(2)}, u32[]{:S(2)}) async-start(s32[8,1,2]{2,1,0:T(1,128)} %copy.21), calls=%async_computation | async-start | bytes 8192 | tf_op jit(solution)/shard_map/all_to_all | solution.py:182
  11.4 2.3 %copy-start.2 = (f32[256]{0:T(256)S(1)}, f32[256]{0:T(256)}, u32[]{:S(2)}) copy-start(f32[256]{0:T(256)} %param.9) | copy-start | bytes 3076
  13.7 13.3 %copy-start.1 = (s32[1792]{0:T(1024)S(1)}, s32[1792]{0:T(1024)}, u32[]{:S(2)}) copy-start(s32[1792]{0:T(1024)} %constant.49.clone.1) | copy-start | bytes 21508
  21.5 19.5 %all-to-all-start.1 = ((bf16[8,2,64,256]{3,2,1,0:T(8,128)(2,1)}), bf16[8,2,64,256]{3,2,1,0:T(8,128)(2,1)}, u32[]{:S(2)}, u32[]{:S(2)}) async-start(bf16[8,2,64,256]{3,2,1,0:T(8,128)(2,1)} %broadcast_select_fusion), calls=%async_computation.1 | async-start | bytes 1048576 | tf_op jit(solution)/shard_map/all_to_all | solution.py:186

commit v2 on v1

v2 whole, which is shorter than its diff:
```python
import functools

import jax
import jax.numpy as jnp
from jax import lax
from jax.experimental import pallas as pl
from jax.experimental.pallas import tpu as pltpu
from jax.sharding import PartitionSpec as P

CAP = 2
PAIR = 2
FAR = 1 << 30
LOG2E = 1.4426950408889634

epsilon = 1e-06


def fused_kernel(
    n_kv, n_tp, blk, heads, rank, per_device, picks, per_shard,
    tok_hbm, wq_hbm, wl_hbm, gain_ref, wo_hbm, chosen_ref, out_ref, log_ref,
    tok, wq, wl, wo, queries, keys, pos_ref, log_buf, req_send, asked, reply,
    heads_buf, own, a_send, a_recv, x_send, x_recv,
    load_sem, req_ss, req_rs, far_ss, far_rs, fwd_ss, fwd_rs, a_ss, a_rs, x_ss, x_rs,
):
    my = lax.axis_index("kv")
    me = lax.axis_index("tp")
    pair, core = me // PAIR, me % PAIR
    groups = n_tp // PAIR
    partner = pair * PAIR + (PAIR - 1 - core)
    steps = groups * per_shard
    scale = rank ** (-0.5)
    factor = scale * LOG2E
    rows = per_device * blk
    half_rows = blk // PAIR
    piece = CAP * half_rows
    chunk = rows // n_tp

    loads = [
        pltpu.make_async_copy(src, dst, load_sem.at[i])
        for i, (src, dst) in enumerate(
            [(tok_hbm, tok), (wl_hbm, wl), (wq_hbm, wq), (wo_hbm, wo)]
        )
    ]
    for load in loads:
        load.start()

    barrier = pltpu.get_barrier_semaphore()

    def greet(o, carry):
        pl.semaphore_signal(barrier, inc=1, device_id={"kv": lax.rem(my + o, n_kv)})
        return carry

    lax.fori_loop(1, n_kv, greet, 0)
    pl.semaphore_signal(barrier, inc=1, device_id={"tp": partner})
    for o in range(1, groups):
        pl.semaphore_signal(
            barrier, inc=1, device_id={"tp": lax.rem(pair + o, groups) * PAIR + core}
        )

    def ask(d, slot):
        return pltpu.make_async_remote_copy(
            src_ref=req_send.at[d], dst_ref=asked.at[slot],
            send_sem=req_ss.at[d], recv_sem=req_rs.at[slot], device_id={"kv": d},
        )

    def far_rows(d, side):
        return pl.ds(pl.multiple_of(rows + (d * PAIR + side) * piece, piece), piece)

    def answer(p, d):
        return pltpu.make_async_remote_copy(
            src_ref=reply.at[p], dst_ref=keys.at[far_rows(d, core)],
            send_sem=far_ss.at[p], recv_sem=far_rs.at[d], device_id={"kv": p},
        )

    def forward(d, side):
        return pltpu.make_async_remote_copy(
            src_ref=keys.at[far_rows(d, side)], dst_ref=keys.at[far_rows(d, side)],
            send_sem=fwd_ss.at[d], recv_sem=fwd_rs.at[d], device_id={"tp": partner},
        )

    lanes = pos_blocks(n_kv * per_device)
    block_ids = lax.broadcasted_iota(jnp.int32, (per_device, lanes), 1)
    named = jnp.zeros((per_device, lanes), jnp.int32)
    for j in range(picks):
        named = jnp.maximum(named, (chosen_ref[:, j:j + 1] == block_ids).astype(jnp.int32))
    wanted = jnp.broadcast_to(jnp.max(named, axis=0, keepdims=True), (8, lanes))
    named = named.astype(jnp.float32).astype(jnp.bfloat16)
    first = lax.broadcasted_iota(jnp.int32, (lanes, lanes), 0)
    second = lax.broadcasted_iota(jnp.int32, (lanes, lanes), 1)
    ahead = (first < second) & (first // per_device == second // per_device)
    counted = jnp.dot(
        wanted.astype(jnp.float32).astype(jnp.bfloat16),
        ahead.astype(jnp.float32).astype(jnp.bfloat16),
        preferred_element_type=jnp.float32,
    ).astype(jnp.int32)
    lane_block = lax.broadcasted_iota(jnp.int32, (8, lanes), 1)
    lane_owner = lane_block // per_device
    slot_of = jnp.where((wanted > 0) & (lane_owner < my), lane_owner * CAP + counted, -1)
    slot_of = jnp.where(counted < CAP, slot_of, -1)
    lane_local = lane_block - lane_owner * per_device

    slot3 = (
        lax.broadcasted_iota(jnp.int32, (n_kv, 8, lanes), 0) * CAP
        + lax.broadcasted_iota(jnp.int32, (n_kv, 8, lanes), 1)
    )
    real3 = lax.broadcasted_iota(jnp.int32, (n_kv, 8, lanes), 1) < CAP
    index3 = jnp.sum(
        jnp.where(real3 & (slot3 == slot_of[None]), lane_local[None], 0), axis=2, keepdims=True
    )
    req_send[...] = jnp.broadcast_to(index3, (n_kv, 8, 128))

    pl.semaphore_wait(barrier, n_kv - 1 + groups)

    def send_ask(d, carry):
        @pl.when(d < my)
        def _():
            ask(d, my).start()

        return carry

    lax.fori_loop(0, n_kv - 1, send_ask, 0)

    own_key = lax.broadcasted_iota(jnp.int32, (lanes, rows), 1)
    own_pick = (lax.broadcasted_iota(jnp.int32, (lanes, rows), 0) - my * per_device) == own_key // blk
    own_named = jnp.dot(
        named, own_pick.astype(jnp.float32).astype(jnp.bfloat16), preferred_element_type=jnp.float32
    )
    place = lax.broadcasted_iota(jnp.int32, (per_device, rows), 1)
    pos_ref[:, :rows] = jnp.where(own_named > 0.5, place, FAR)
    slots = n_kv * CAP
    match = (
        jnp.broadcast_to(slot_of[:1], (slots, lanes))
        == lax.broadcasted_iota(jnp.int32, (slots, lanes), 0)
    )
    slot_named = lax.dot_general(
        named, match.astype(jnp.float32).astype(jnp.bfloat16), (((1,), (1,)), ((), ())),
        preferred_element_type=jnp.float32,
    )
    far_count = (n_kv - 1) * CAP * blk
    far_key = lax.broadcasted_iota(jnp.int32, (slots, far_count), 1)
    key_slot = far_key // (CAP * blk) * CAP + far_key // half_rows % CAP
    spread = key_slot == lax.broadcasted_iota(jnp.int32, (slots, far_count), 0)
    far_named = jnp.dot(
        slot_named.astype(jnp.bfloat16), spread.astype(jnp.float32).astype(jnp.bfloat16),
        preferred_element_type=jnp.float32,
    )
    pos_ref[:, rows:] = jnp.where(far_named > 0.5, -1, FAR)

    loads[0].wait()
    loads[1].wait()

    def latent_rows(i, carry):
        span = pl.ds(pl.multiple_of(i * chunk, chunk), chunk)
        projected = jnp.dot(tok[span, :], wl[...], preferred_element_type=jnp.float32)
        inv_rms = lax.rsqrt(jnp.mean(projected * projected, axis=-1, keepdims=True) + epsilon)
        keys[span, :] = (projected * inv_rms * gain_ref[...]).astype(jnp.bfloat16)
        return carry

    lax.fori_loop(0, n_tp, latent_rows, 0)

    def send_reply(o, carry):
        p = my + (n_kv - o)

        @pl.when(p < n_kv)
        def _():
            ask(my, p).wait_recv()
            want = asked[p]
            within = core * half_rows + lax.broadcasted_iota(jnp.int32, (half_rows, 1), 0)
            source = jnp.concatenate(
                [want[c:c + 1, :1] * blk + within for c in range(CAP)], axis=0
            )
            pick = lax.broadcasted_iota(jnp.int32, (piece, rows), 1) == source
            reply[p] = jnp.dot(
                pick.astype(jnp.float32).astype(jnp.bfloat16), keys[:rows, :],
                preferred_element_type=jnp.float32,
            ).astype(jnp.bfloat16)
            answer(p, my).start()

        return carry

    lax.fori_loop(1, n_kv, send_reply, 0)
    loads[2].wait()

    def query_rows(i, carry):
        span = pl.ds(pl.multiple_of(i * chunk, chunk), chunk)
        queries[span, :] = jnp.dot(
            tok[span, :], wq[...], preferred_element_type=jnp.float32
        ).astype(jnp.bfloat16)
        return carry

    def pass_on(d, carry):
        @pl.when(d < my)
        def _():
            answer(my, d).wait_recv()
            forward(d, core).start()

        @pl.when(d >= my)
        def _():
            whole = pl.ds(pl.multiple_of(rows + d * CAP * blk, CAP * blk), CAP * blk)
            keys[whole, :] = jnp.zeros((CAP * blk, rank), jnp.bfloat16)

        return carry

    def take_passed(d, carry):
        @pl.when(d < my)
        def _():
            forward(d, PAIR - 1 - core).wait_recv()

        return carry

    lax.fori_loop(0, n_tp - 1, query_rows, 0)
    lax.fori_loop(0, n_kv - 1, pass_on, 0)
    query_rows(n_tp - 1, 0)
    lax.fori_loop(0, n_kv - 1, take_passed, 0)
    loads[3].wait()

    def near(s):
        return pltpu.make_async_remote_copy(
            src_ref=a_send.at[s], dst_ref=a_recv.at[s],
            send_sem=a_ss.at[s], recv_sem=a_rs.at[s], device_id={"tp": partner},
        )

    def cross(s):
        peer = lax.rem(pair + 1 + s // per_shard, groups) * PAIR + core
        return pltpu.make_async_remote_copy(
            src_ref=x_send.at[s], dst_ref=x_recv.at[s],
            send_sem=x_ss.at[s], recv_sem=x_rs.at[s], device_id={"tp": peer},
        )

    def attend(g, half):
        row0 = pl.multiple_of(g * blk, blk)
        q = jnp.concatenate(
            [queries[pl.ds(row0, blk), h * rank:(h + 1) * rank] for h in range(heads)], axis=0
        )
        table = keys[...]
        s = lax.dot_general(q, table, (((1,), (1,)), ((), ())), preferred_element_type=jnp.float32)
        pos = pos_ref[pl.ds(g, 1), :]
        query_pos = g * blk + lax.rem(
            lax.broadcasted_iota(jnp.int32, (heads * blk, 1), 0), jnp.int32(blk)
        )
        s = jnp.where(pos <= query_pos, s, -jnp.inf)
        peak = jnp.max(s, axis=1, keepdims=True)
        p = jnp.exp2((s - peak) * factor)
        mass = jnp.sum(p, axis=1, keepdims=True)
        summed = jnp.dot(p.astype(jnp.bfloat16), table, preferred_element_type=jnp.float32)
        result = (summed / mass).astype(jnp.bfloat16)
        logs = peak * scale + jnp.log(mass)
        for h in range(heads):
            heads_buf[half * blk:(half + 1) * blk, h * rank:(h + 1) * rank] = (
                result[h * blk:(h + 1) * blk]
            )
        log_buf[pl.ds(row0, blk), :] = jnp.concatenate(
            [logs[h * blk:(h + 1) * blk] for h in range(heads)]
            + [jnp.zeros((blk, 128 - heads), jnp.float32)],
            axis=1,
        )

    def finish(s):
        near(s).wait_recv()
        total = own[s] + a_recv[s].astype(jnp.float32)

        @pl.when(s < steps - per_shard)
        def _():
            x_send[s] = total.astype(jnp.bfloat16)
            cross(s).start()

        @pl.when(s >= steps - per_shard)
        def _():
            own[s] = total

    def step(s, carry):
        group = lax.rem(pair + 1 + s // per_shard, groups)
        inner = lax.rem(s, per_shard)
        attend((group * PAIR + (PAIR - 1 - core)) * per_shard + inner, 0)
        attend((group * PAIR + core) * per_shard + inner, 1)
        part = jnp.dot(heads_buf[...], wo[...], preferred_element_type=jnp.float32)
        a_send[s] = part[:blk].astype(jnp.bfloat16)
        own[s] = part[blk:]
        near(s).start()

        @pl.when(s >= 1)
        def _():
            finish(s - 1)

        return carry

    lax.fori_loop(0, steps, step, 0)
    finish(steps - 1)
    for i in range(per_shard):
        total = own[steps - per_shard + i]
        for o in range(groups - 1):
            slot = o * per_shard + i
            cross(slot).wait_recv()
            total = total + x_recv[slot].astype(jnp.float32)
        out_ref[i * blk:(i + 1) * blk, :] = total.astype(jnp.bfloat16)
    for s in range(steps):
        near(s).wait_send()
    for s in range(steps - per_shard):
        cross(s).wait_send()
    log_ref[...] = log_buf[...].T[:heads]

    def drain(d, carry):
        @pl.when(d < my)
        def _():
            ask(d, my).wait_send()
            forward(d, core).wait_send()

        @pl.when(d + 1 > my)
        def _():
            answer(d + 1, my).wait_send()

        return carry

    lax.fori_loop(0, n_kv - 1, drain, 0)


def pos_blocks(count):
    return -(-count // 128) * 128


def local(tokens, w_query, w_latent, latent_gain, w_output, chosen):
    rows, width = tokens.shape[0], w_output.shape[1]
    rank = w_latent.shape[1]
    heads = w_query.shape[1] // rank
    per_device, picks = chosen.shape
    blk = rows // per_device
    n_kv, n_tp = lax.axis_size("kv"), lax.axis_size("tp")
    per_shard = per_device // n_tp
    steps = (n_tp // PAIR) * per_shard
    crossing = steps - per_shard
    n_keys = rows + (n_kv - 1) * CAP * blk
    piece = CAP * (blk // PAIR)
    any_spec = pl.BlockSpec(memory_space=pl.ANY)
    vmem_spec = pl.BlockSpec(memory_space=pltpu.VMEM)
    attended, log_rows = pl.pallas_call(
        functools.partial(
            fused_kernel, n_kv, n_tp, blk, heads, rank, per_device, picks, per_shard
        ),
        out_shape=(
            jax.ShapeDtypeStruct((rows // n_tp, width), jnp.bfloat16),
            jax.ShapeDtypeStruct((heads, rows), jnp.float32),
        ),
        in_specs=[any_spec, any_spec, any_spec, vmem_spec, any_spec, vmem_spec],
        out_specs=[vmem_spec, vmem_spec],
        scratch_shapes=[
            pltpu.VMEM(tokens.shape, jnp.bfloat16),
            pltpu.VMEM(w_query.shape, jnp.bfloat16),
            pltpu.VMEM(w_latent.shape, jnp.bfloat16),
            pltpu.VMEM(w_output.shape, jnp.bfloat16),
            pltpu.VMEM((rows, heads * rank), jnp.bfloat16),
            pltpu.VMEM((n_keys, rank), jnp.bfloat16),
            pltpu.VMEM((per_device, n_keys), jnp.int32),
            pltpu.VMEM((rows, 128), jnp.float32),
            pltpu.VMEM((n_kv, 8, 128), jnp.int32),
            pltpu.VMEM((n_kv, 8, 128), jnp.int32),
            pltpu.VMEM((n_kv, piece, rank), jnp.bfloat16),
            pltpu.VMEM((PAIR * blk, heads * rank), jnp.bfloat16),
            pltpu.VMEM((steps, blk, width), jnp.float32),
            pltpu.VMEM((steps, blk, width), jnp.bfloat16),
            pltpu.VMEM((steps, blk, width), jnp.bfloat16),
            pltpu.VMEM((crossing, blk, width), jnp.bfloat16),
            pltpu.VMEM((crossing, blk, width), jnp.bfloat16),
            pltpu.SemaphoreType.DMA((4,)),
        ]
        + [pltpu.SemaphoreType.DMA((n_kv,))] * 6
        + [pltpu.SemaphoreType.DMA((steps,))] * 2
        + [pltpu.SemaphoreType.DMA((crossing,))] * 2,
        compiler_params=pltpu.CompilerParams(
            collective_id=0, has_side_effects=True, vmem_limit_bytes=60 * 1024 * 1024
        ),
    )(tokens, w_query, w_latent, latent_gain[None, :], w_output, chosen)
    return attended, log_rows.T


def solution(mesh):
    placed = (P("kv", None), P(None, "tp"), P(), P(), P("tp", None), P("kv", None))
    return jax.shard_map(
        local,
        mesh=mesh,
        in_specs=placed,
        out_specs=(P(("kv", "tp"), None), P("kv", "tp")),
        check_vma=False,
    )
```

time: 77.3 us -> 45.3 us (0.59)
  starting transfers between devices: 12.8 us -> 0 us
  Pallas kernels: 29.7 us -> 40.8 us
  matrix products: 8.97 us -> 0 us
  other arithmetic: 8.7 us -> 0 us
  waiting for transfers between devices: 6.52 us -> 0 us
  local copies, waits for them, and re-layouts: 9.22 us -> 3.4 us
    all_to_all x2 -> x0, starting transfers between devices: 12.8 us -> none  [the longest x1 7.31 us: local(): lax.all_to_all(request, 'kv', split_axis=0, concat_axis=0, tiled=True)]
    pallas_call x1, Pallas kernels: 29.7 us -> 40.8 us  [local(): pl.pallas_call(functools.partial(fused_kernel, n_kv, n_tp, blk, heads, ra...]
    dot_general x2 -> x0, matrix products: 8.97 us -> none  [the longest x1 6.68 us: local(): jnp.dot(tokens, w_query, preferred_element_type=jnp.float32)]
    all_to_all x2 -> x0, waiting for transfers between devices: 6.52 us -> none  [the longest x1 5.99 us: local(): lax.all_to_all(reply_blocks, 'kv', split_axis=0, concat_axis=0, tiled=True)]
    select_n x3 -> x0, other arithmetic: 3.35 us -> none  [the longest x1 1.95 us: local(): reply_blocks = jnp.take(own_blocks, jnp.maximum(asked, 0), axis=0)]
    concatenate x2 -> x0, other arithmetic: 2.1 us -> none  [the longest x1 2.03 us: local(): jnp.concatenate([latent, fetched.reshape(devices * CAP * blk_len, lat_ran...]
    reduce_or x3 -> x0, other arithmetic: 1.97 us -> none  [the longest x1 0.98 us: local(): wanted = jnp.any(named, axis=0).reshape(devices, per_device)]
    pallas_call x1 -> x0, local copies, waits for them, and re-layouts: 1.75 us -> none  [attend_and_reduce(): pl.pallas_call(functools.partial(attend_kernel, n_tp, blk, heads, rank, p...]
  transfers between devices with their start and end apart: 2 -> 0, of which waited for: 2 -> 0; matrix products, arithmetic and copies ran while one was open for 18% -> 0% of each run, Pallas kernels for 0% -> 0%
where the time goes in v2:
time: 45.3 us; the launch traced here: 44.9 us
  Pallas kernels  40.8 us (90%)
  local copies, waits for them, and re-layouts  3.4 us (8%)
  between operations  0.64 us (1%)
    pallas_call x1, Pallas kernels, local(): pl.pallas_call(functools.partial(fused_kernel, n_kv, n_tp, blk, heads, ra...  40.8 us
    unnamed x2, local copies, waits for them, and re-layouts  3.4 us

profile of v2, /device:TPU:0, one launch (start us, length us, event | category | flops | bytes accessed | tf_op | source)
XLA Modules:
  0.0 44.9 jit_solution(14918706453742081253)
XLA Ops:
  0.6 40.8 %shard_map.77 = (bf16[192,2048]{1,0:T(8,128)(2,1)}, f32[4,768]{1,0:T(4,128)}) custom-call(bf16[768,2048]{1,0:T(8,128)(2,1)} %tok_hbm.1, bf16[2048,1024]{1,0:T(8,128)(2,1)} %wq_hbm.1, bf16[2048,256]{1,0:T(8,128)(2,1)} %wl_hbm.1, f32[1,256]{1,0:T(1,128)} %bitcast.3, bf16[1024,2048]{1,0:T(8,128)(2,1)} %wo_hbm.1, s32[12,32]{1,0:T(8,128)} %chosen_ref.1), custom_call_target="tpu_custom_call" | custom-call | tf_op jit(solution)/shard_map/pallas_call | solution.py:335
  41.5 2.1 %copy.10 = bf16[192,2048]{1,0:T(8,128)(2,1)} copy(bf16[192,2048]{1,0:T(8,128)(2,1)} %get-tuple-element.8) | data formatting | bytes 1572864
  43.6 1.3 %copy.11 = f32[768,4]{0,1:T(4,128)} copy(f32[768,4]{0,1:T(4,128)} %bitcast.2) | data formatting | bytes 24576
